TPU v7x, 32 devices: a whole 2x2x4 slice. The times are simulated.
32 devices in a mesh: sp: 8 (over z, y), tp: 4 (over x, core).
Axes of the slice: x: 2, y: 2, z: 4, core: 2. Of those that a mesh axis runs over, the one named last changes fastest.
Arguments:
- resid: bfloat16 [2048, 2048], P(('sp', 'tp')), may hold values from -6 to 6
- query_a: bfloat16 [2048, 4, 128], P('sp', 'tp')
- key_a: bfloat16 [2048, 4, 128], P('sp', 'tp')
- value_a: bfloat16 [2048, 4, 128], P('sp', 'tp'), may hold values from -6 to 6
- query_b: bfloat16 [2048, 4, 256], P('sp', 'tp')
- key_b: bfloat16 [2048, 4, 256], P('sp', 'tp')
- value_b: bfloat16 [2048, 4, 128], P('sp', 'tp'), may hold values from -6 to 6
- lambda_a: float32 [4], P('tp'), may hold values from 0.3 to 0.8
- lambda_b: float32 [4], P('tp'), may hold values from 0.3 to 0.8
- head_gain: float32 [128], replicated, may hold values from 0.1 to 1.9
- out_weight: bfloat16 [1024, 2048], replicated, may hold values from -0.1875 to 0.1875
- norm_gain: float32 [2048], replicated, may hold values from 0.1 to 1.9
- expert_ids: int32 [2048, 4], P(('sp', 'tp')), may hold values from 0 to 31, all different within a row; in each aligned block of 64 rows (0 to 63, 64 to 127, ...) at most 16 rows name the same one
- expert_mix: float32 [2048, 4], P(('sp', 'tp')), may hold values from 0.2 to 1
- gate_experts: bfloat16 [32, 2048, 1024], P(('sp', 'tp')), may hold values from -0.125 to 0.125
- up_experts: bfloat16 [32, 2048, 1024], P(('sp', 'tp')), may hold values from -0.125 to 0.125
- down_experts: bfloat16 [32, 1024, 2048], P(('sp', 'tp')), may hold values from -0.1875 to 0.1875
- shared_gate: bfloat16 [2048, 512], replicated, may hold values from -0.125 to 0.125
- shared_up: bfloat16 [2048, 512], replicated, may hold values from -0.125 to 0.125
- shared_down: bfloat16 [512, 2048], replicated, may hold values from -0.25 to 0.25
Outputs:
- layer_out: bfloat16 [2048, 2048], P(('sp', 'tp'))
Inputs may be any that keep to these rules, and one draw needn't show every extreme that they name: `expert_ids`: in each aligned block of 64 rows (the rows of one device) no expert is named more than 16 times, a bound that some block reaches.
All inputs are finite; a program needn't handle non-finite values.
Results may differ from a plain program's by a relative error of at most 0.017.
Values may be sent and summed in bfloat16 or wider, within the bound.
No kernel may reach another device: no remote copies, remote signals or barrier semaphores. Data moves between devices by JAX's collectives and lax.ppermute only.
A program may use at most 128 MiB of HBM per device.

v0:
```python
import math

import jax
import jax.numpy as jnp
from jax import lax
from jax.sharding import PartitionSpec as P

NEG_FILL = -1e30
EPSILON = 1e-05
HEAD_SCALE = 0.8
KEY_SPAN = 2048


def swiglu_rows(row_set, w_gate, w_up, w_down):
    gate_val = jnp.dot(row_set, w_gate, preferred_element_type=jnp.float32)
    up_val = jnp.dot(row_set, w_up, preferred_element_type=jnp.float32)
    hidden = (jax.nn.silu(gate_val) * up_val).astype(jnp.bfloat16)
    return jnp.dot(hidden, w_down, preferred_element_type=jnp.float32)


def online_update(state, query_map, key_map, value_block, causal, scaling):
    row_top, denoms, numerator = state
    scores = (
        jnp.einsum("qhd,khd->hqk", query_map, key_map, preferred_element_type=jnp.float32) * scaling
    )
    scores = jnp.where(causal, scores, NEG_FILL)
    new_top = jnp.maximum(row_top, jnp.max(scores, axis=2))
    exponent = jnp.where(causal, jnp.exp(scores - new_top[:, :, None]), 0.0)
    shrink = jnp.exp(row_top - new_top)
    denoms = denoms * shrink + jnp.sum(exponent, axis=2)
    numerator = numerator * jnp.transpose(shrink)[:, :, None] + jnp.einsum(
        "hqk,khe->qhe",
        exponent.astype(jnp.bfloat16),
        value_block,
        preferred_element_type=jnp.float32,
    )
    return (new_top, denoms, numerator)


def group_update(states, queries, key_block, value_block, causal):
    map_width = queries.shape[2] // 2
    scaling = map_width ** (-0.5)
    first_state = online_update(
        states[0],
        queries[:, :, :map_width],
        key_block[:, :, :map_width],
        value_block,
        causal,
        scaling,
    )
    second_state = online_update(
        states[1],
        queries[:, :, map_width:],
        key_block[:, :, map_width:],
        value_block,
        causal,
        scaling,
    )
    return (first_state, second_state)


def empty_state(query_rows, head_count, value_width):
    single = (
        jnp.full((head_count, query_rows), NEG_FILL, jnp.float32),
        jnp.zeros((head_count, query_rows), jnp.float32),
        jnp.zeros((query_rows, head_count, value_width), jnp.float32),
    )
    return (single, single)


def finish_group(states, lambdas, head_gain):
    first_out = states[0][2] / jnp.transpose(states[0][1])[:, :, None]
    second_out = states[1][2] / jnp.transpose(states[1][1])[:, :, None]
    differ = first_out - lambdas[None, :, None] * second_out
    scale_rms = lax.rsqrt(jnp.mean(differ * differ, axis=2, keepdims=True) + EPSILON)
    return (differ * scale_rms * head_gain[None, None, :] * HEAD_SCALE).astype(jnp.bfloat16)


def per_device(
    resid,
    query_a,
    key_a,
    value_a,
    query_b,
    key_b,
    value_b,
    lambda_a,
    lambda_b,
    head_gain,
    out_weight,
    norm_gain,
    expert_ids,
    expert_mix,
    gate_experts,
    up_experts,
    down_experts,
    shared_gate,
    shared_up,
    shared_down,
):
    query_rows = query_a.shape[0]
    value_width = value_a.shape[2]
    query_pos = lax.axis_index("sp") * query_rows + jnp.arange(query_rows, dtype=jnp.int32)
    start_state = (
        empty_state(query_rows, query_a.shape[1], value_width),
        empty_state(query_rows, query_b.shape[1], value_width),
    )
    key_piece_a = lax.all_gather(key_a, "sp", axis=0, tiled=True)
    value_piece_a = lax.all_gather(value_a, "sp", axis=0, tiled=True)
    key_piece_b = lax.all_gather(key_b, "sp", axis=0, tiled=True)
    value_piece_b = lax.all_gather(value_b, "sp", axis=0, tiled=True)
    piece_rows = key_piece_a.shape[0]
    step_rows = math.gcd(piece_rows, KEY_SPAN)

    def one_step(step_index, inner_state):
        begin_row = step_index * step_rows
        key_pos = begin_row + jnp.arange(step_rows, dtype=jnp.int32)
        causal = (key_pos[None, :] <= query_pos[:, None])[None]
        part_a = group_update(
            inner_state[0],
            query_a,
            lax.dynamic_slice_in_dim(key_piece_a, begin_row, step_rows, 0),
            lax.dynamic_slice_in_dim(value_piece_a, begin_row, step_rows, 0),
            causal,
        )
        part_b = group_update(
            inner_state[1],
            query_b,
            lax.dynamic_slice_in_dim(key_piece_b, begin_row, step_rows, 0),
            lax.dynamic_slice_in_dim(value_piece_b, begin_row, step_rows, 0),
            causal,
        )
        return (part_a, part_b)

    state_a, state_b = lax.fori_loop(0, piece_rows // step_rows, one_step, start_state)
    heads_a = finish_group(state_a, lambda_a, head_gain)
    heads_b = finish_group(state_b, lambda_b, head_gain)
    tok_dev = resid.shape[0]
    back_a, back_b = (
        lax.all_to_all(heads_a, "tp", split_axis=0, concat_axis=1, tiled=True),
        lax.all_to_all(heads_b, "tp", split_axis=0, concat_axis=1, tiled=True),
    )
    joined = jnp.concatenate([back_a.reshape(tok_dev, -1), back_b.reshape(tok_dev, -1)], axis=1)
    project = jnp.dot(joined, out_weight, preferred_element_type=jnp.float32)
    middle = (resid.astype(jnp.float32) + project).astype(jnp.bfloat16)
    middle_f = middle.astype(jnp.float32)
    normed = (
        middle_f
        * lax.rsqrt(jnp.mean(middle_f * middle_f, axis=1, keepdims=True) + EPSILON)
        * norm_gain[None, :]
    ).astype(jnp.bfloat16)
    shared = swiglu_rows(normed, shared_gate, shared_up, shared_down)
    top_count = expert_ids.shape[1]
    model_width = normed.shape[1]
    sp_count = lax.axis_size("sp")
    tp_count = lax.axis_size("tp")
    expert_total = sp_count * tp_count
    pair_count = tok_dev * top_count
    capacity = max(2, 2 * pair_count // expert_total)
    flat_ids = expert_ids.reshape(-1)
    one_hot = (flat_ids[:, None] == jnp.arange(expert_total, dtype=jnp.int32)[None, :]).astype(
        jnp.int32
    )
    pair_rank = jnp.sum((jnp.cumsum(one_hot, axis=0) - one_hot) * one_hot, axis=1)
    pair_token = jnp.arange(pair_count, dtype=jnp.int32) // top_count
    send_rows = (
        jnp.zeros((expert_total, capacity, model_width), jnp.bfloat16)
        .at[flat_ids, pair_rank]
        .set(normed[pair_token])
    )
    arrived = lax.all_to_all(send_rows, ("sp", "tp"), split_axis=0, concat_axis=0, tiled=True)
    arrived_shape = arrived.shape
    flat_rows = arrived.reshape(-1, arrived_shape[-1])
    result = swiglu_rows(flat_rows, gate_experts[0], up_experts[0], down_experts[0]).astype(
        jnp.bfloat16
    )
    finished = result.reshape(arrived_shape)
    returned = lax.all_to_all(finished, ("sp", "tp"), split_axis=0, concat_axis=0, tiled=True)
    chosen = returned[flat_ids, pair_rank].reshape(tok_dev, top_count, model_width)
    routed = jnp.sum(chosen.astype(jnp.float32) * expert_mix[:, :, None], axis=1)
    return (middle_f + shared + routed).astype(jnp.bfloat16)


def solution(mesh):
    in_specs = (
        P(("sp", "tp"), None),
        P("sp", "tp", None),
        P("sp", "tp", None),
        P("sp", "tp", None),
        P("sp", "tp", None),
        P("sp", "tp", None),
        P("sp", "tp", None),
        P("tp"),
        P("tp"),
        P(),
        P(),
        P(),
        P(("sp", "tp"), None),
        P(("sp", "tp"), None),
        P(("sp", "tp"), None, None),
        P(("sp", "tp"), None, None),
        P(("sp", "tp"), None, None),
        P(),
        P(),
        P(),
    )
    out_specs = P(("sp", "tp"), None)
    return jax.shard_map(
        per_device, mesh=mesh, in_specs=in_specs, out_specs=out_specs, check_vma=False
    )
```

profile of v0, /device:TPU:0, one launch (start us, length us, event | category | flops | bytes accessed | tf_op | source)
XLA Modules:
  0.0 333.9 jit_solution(18437636033774966400)
XLA Ops:
  6.5 0.7 all-gather.2.cloned.1.call-update
  7.3 33.6 %all_gather.12 = bf16[2048,1,128]{2,0,1:T(8,128)(2,1)S(1)} all-gather(bf16[256,1,128]{2,0,1:T(8,128)(2,1)} %param.22), channel_id=1, replica_groups=mesh['sp'=8,'tp'=4] {'sp'}, dimensions={0}, use_global_device_ids=true | all-gather | bytes 589824 | tf_op jit(solution)/shard_map/all_gather | solution.py:108
  40.9 0.8 copy.35
  44.2 2.8 fusion.88
  47.0 1.8 fusion.89
  48.9 31.4 %all_gather.15 = bf16[2048,1,128]{2,0,1:T(8,128)(2,1)S(1)} all-gather(bf16[256,1,128]{2,0,1:T(8,128)(2,1)S(1)} %copy-done.5), channel_id=1, replica_groups=mesh['sp'=8,'tp'=4] {'sp'}, dimensions={0}, use_global_device_ids=true | all-gather | bytes 589824 | tf_op jit(solution)/shard_map/all_gather | solution.py:111
  80.3 31.5 %all_gather.13 = bf16[2048,1,128]{2,0,1:T(8,128)(2,1)S(1)} all-gather(bf16[256,1,128]{2,0,1:T(8,128)(2,1)S(1)} %copy-done.6), channel_id=1, replica_groups=mesh['sp'=8,'tp'=4] {'sp'}, dimensions={0}, use_global_device_ids=true | all-gather | bytes 589824 | tf_op jit(solution)/shard_map/all_gather | solution.py:109
  111.8 1.8 fusion.91
  113.6 1.8 fusion.90
  115.4 2.1 fusion.19
  121.0 0.7 reduce.22
  122.5 3.3 all-to-all-start.1
  125.8 0.7 reduce.23
  127.3 2.6 all-to-all-done.1
  129.9 3.3 all-to-all-start
  133.3 3.9 %all-to-all-done = bf16[4,2,4096]{2,1,0:T(2,128)(2,1)S(1)} async-done(((bf16[4,2,4096]{2,1,0:T(2,128)(2,1)}), bf16[4,2,4096]{2,1,0:T(2,128)(2,1)S(1)}, u32[]{:S(2)}, u32[]{:S(2)}) %all-to-all-start) | async-done | bytes 65568 | tf_op jit(solution)/shard_map/all_to_all | solution.py:140
  137.4 3.2 multiply_reduce_fusion.1
  140.7 2.3 gather_fusion
  143.1 1.6 broadcast_in_dim.49
  144.7 46.3 %scatter_fusion = bf16[32,16,2048]{2,1,0:T(8,128)(2,1)} fusion(bf16[32,16,2048]{2,1,0:T(8,128)(2,1)} %broadcast_in_dim.49, s32[256]{0:T(256)S(1)} %bitcast.169, bf16[256,2048]{1,0:T(8,128)(2,1)} %gather_fusion), kind=kCustom, calls=%fused_computation.2 | custom fusion | bytes 3147776 | tf_op jit(solution)/shard_map/scatter | solution.py:169
  191.0 53.6 %all_to_all.40 = bf16[32,16,2048]{2,1,0:T(8,128)(2,1)S(1)} all-to-all(bf16[32,16,2048]{2,1,0:T(8,128)(2,1)} %scatter_fusion), channel_id=1, replica_groups=mesh['sp'=8,'tp'=4] {'sp','tp'}, dimensions={0} | all-to-all | bytes 4194304 | tf_op jit(solution)/shard_map/all_to_all | solution.py:171
  244.6 1.3 copy-done.3
  245.9 3.6 %fusion.4 = f32[512,1024]{1,0:T(8,128)} fusion(bf16[512,2048]{1,0:T(8,128)(2,1)S(1)} %bitcast.171, bf16[1,2048,1024]{2,1,0:T(8,128)(2,1)S(1)} %copy-done.10), kind=kOutput, calls=%fused_computation.7 | convolution fusion | flops 2147483648 | bytes 8388608 | tf_op jit(solution)/shard_map/dot_general | solution.py:15
  249.6 10.6 %fusion.6 = bf16[512,2048]{1,0:T(8,128)(2,1)} fusion(bf16[1,1024,2048]{2,1,0:T(8,128)(2,1)} %param.36, f32[512,1024]{1,0:T(8,128)} %fusion.4, bf16[512,2048]{1,0:T(8,128)(2,1)} %bitcast.172, bf16[1,2048,1024]{2,1,0:T(8,128)(2,1)} %param.35), kind=kOutput, calls=%fused_computation.9 | convolution fusion | flops 4299161600 | bytes 14680064 | tf_op jit(solution)/shard_map/dot_general | solution.py:18
  260.2 3.8 %all-to-all-start.3 = ((bf16[32,16,2048]{2,1,0:T(8,128)(2,1)}), bf16[32,16,2048]{2,1,0:T(8,128)(2,1)}, u32[]{:S(2)}, u32[]{:S(2)}) async-start(bf16[32,16,2048]{2,1,0:T(8,128)(2,1)} %bitcast.170), calls=%async_computation.3 | async-start | bytes 4194304 | tf_op jit(solution)/shard_map/all_to_all | solution.py:178
  264.0 0.7 copy.39
  264.7 2.1 fusion.92
  266.8 45.9 %all-to-all-done.3 = bf16[32,16,2048]{2,1,0:T(8,128)(2,1)} async-done(((bf16[32,16,2048]{2,1,0:T(8,128)(2,1)}), bf16[32,16,2048]{2,1,0:T(8,128)(2,1)}, u32[]{:S(2)}, u32[]{:S(2)}) %all-to-all-start.3) | async-done | bytes 2097184 | tf_op jit(solution)/shard_map/all_to_all | solution.py:178
  312.7 5.1 %gather_fusion.1 = bf16[256,2048]{1,0:T(8,128)(2,1)} fusion(bf16[32,16,2048]{2,1,0:T(8,128)(2,1)} %all-to-all-done.3, s32[256]{0:T(256)S(1)} %bitcast.168), kind=kCustom, calls=%fused_computation.1 | custom fusion | bytes 2099200 | tf_op jit(solution)/shard_map/gather | solution.py:179
  317.8 2.7 reshape.410
  320.6 3.2 multiply_reduce_fusion
  323.8 3.2 fusion.14
  (68 shorter events, 6.7 us)
Async XLA Ops:
  6.5 317.2 %copy-start = (bf16[512,2048]{1,0:T(8,128)(2,1)S(1)}, bf16[512,2048]{1,0:T(8,128)(2,1)}, u32[]{:S(2)}) copy-start(bf16[512,2048]{1,0:T(8,128)(2,1)} %param.39) | copy-start | bytes 6291460
  6.5 40.5 %copy-start.12 = (bf16[256,1,128]{2,0,1:T(8,128)(2,1)S(1)}, bf16[256,1,128]{2,0,1:T(8,128)(2,1)}, u32[]{:S(2)}) copy-start(bf16[256,1,128]{2,0,1:T(8,128)(2,1)} %param.21) | copy-start | bytes 196612
  6.5 105.2 %all-gather.2.cloned.1.call-start = ((), (), s32[]{:S(2)}) async-start(), calls=%async_computation.4 | async-start | bytes 1179648 | tf_op jit(solution)/shard_map/all_gather | solution.py:110
  47.0 1.9 copy-start.5
  47.0 33.3 %copy-start.6 = (bf16[256,1,128]{2,0,1:T(8,128)(2,1)S(1)}, bf16[256,1,128]{2,0,1:T(8,128)(2,1)}, u32[]{:S(2)}) copy-start(bf16[256,1,128]{2,0,1:T(8,128)(2,1)} %param.23) | copy-start | bytes 196612
  47.0 64.8 %copy-start.11 = (bf16[256,1,256]{2,0,1:T(8,128)(2,1)S(1)}, bf16[256,1,256]{2,0,1:T(8,128)(2,1)}, u32[]{:S(2)}) copy-start(bf16[256,1,256]{2,0,1:T(8,128)(2,1)} %param.24) | copy-start | bytes 393220
  111.8 3.6 %copy-start.2 = (f32[256,2048]{1,0:T(8,128)S(1)}, f32[256,2048]{1,0:T(8,128)}, u32[]{:S(2)}) copy-start(f32[256,2048]{1,0:T(8,128)} %get-tuple-element.62) | copy-start | bytes 6291460
  113.6 1.8 copy-start.1
  119.6 0.7 copy-start.9
  120.3 17.1 %copy-start.4 = (bf16[64,2048]{1,0:T(8,128)(2,1)S(1)}, bf16[64,2048]{1,0:T(8,128)(2,1)}, u32[]{:S(2)}) copy-start(bf16[64,2048]{1,0:T(8,128)(2,1)} %param.20) | copy-start | bytes 786436
  122.5 7.4 %all-to-all-start.1 = ((bf16[4,2,4096]{2,1,0:T(2,128)(2,1)}), bf16[4,2,4096]{2,1,0:T(2,128)(2,1)S(1)}, u32[]{:S(2)}, u32[]{:S(2)}) async-start(bf16[4,2,4096]{2,1,0:T(2,128)(2,1)} %reshape.432), calls=%async_computation.1 | async-start | bytes 131072 | tf_op jit(solution)/shard_map/all_to_all | solution.py:141
  129.9 7.4 %all-to-all-start = ((bf16[4,2,4096]{2,1,0:T(2,128)(2,1)}), bf16[4,2,4096]{2,1,0:T(2,128)(2,1)S(1)}, u32[]{:S(2)}, u32[]{:S(2)}) async-start(bf16[4,2,4096]{2,1,0:T(2,128)(2,1)} %reshape.434), calls=%async_computation | async-start | bytes 131072 | tf_op jit(solution)/shard_map/all_to_all | solution.py:140
  137.4 3.2 copy-start.7
  191.0 54.9 %copy-start.10 = (bf16[1,2048,1024]{2,1,0:T(8,128)(2,1)S(1)}, bf16[1,2048,1024]{2,1,0:T(8,128)(2,1)}, u32[]{:S(2)}) copy-start(bf16[1,2048,1024]{2,1,0:T(8,128)(2,1)} %param.34) | copy-start | bytes 12582916
  244.6 1.3 copy-start.3
  260.2 3.8 %copy-start.8 = (f32[64,4]{0,1:T(4,128)S(1)}, f32[64,4]{0,1:T(4,128)}, u32[]{:S(2)}) copy-start(f32[64,4]{0,1:T(4,128)} %param.33) | copy-start | bytes 3076
  260.2 52.5 %all-to-all-start.3 = ((bf16[32,16,2048]{2,1,0:T(8,128)(2,1)}), bf16[32,16,2048]{2,1,0:T(8,128)(2,1)}, u32[]{:S(2)}, u32[]{:S(2)}) async-start(bf16[32,16,2048]{2,1,0:T(8,128)(2,1)} %bitcast.170), calls=%async_computation.3 | async-start | bytes 4194304 | tf_op jit(solution)/shard_map/all_to_all | solution.py:178
Sparse Core Ops, SparseCore 0:
  9.5 43.6 all-gather.1
where the time goes:
time: 336 us; the launch traced here: 334 us
  blocking collectives  150 us (45%)
  local copies, waits for them, and re-layouts  63.9 us (19%)
  waiting for transfers between devices  53.1 us (16%)
  matrix products  33.6 us (10%)
  between operations  15.1 us (4%)
  starting transfers between devices  10.4 us (3%)
  other arithmetic  7.7 us (2%)
    all_to_all x1, blocking collectives, per_device(): lax.all_to_all(send_rows, ('sp', 'tp'), split_axis=0, concat_axis=0, tile...  53.6 us
    scatter x1, local copies, waits for them, and re-layouts, per_device(): send_rows = jnp.zeros((expert_total, capacity, model_width), jnp.bfloat16...  46.3 us
    all_to_all x1, waiting for transfers between devices, per_device(): lax.all_to_all(finished, ('sp', 'tp'), split_axis=0, concat_axis=0, tiled...  45.9 us
    all_gather x1, blocking collectives, per_device(): key_piece_a = lax.all_gather(key_a, 'sp', axis=0, tiled=True)  33.6 us
    all_gather x1, blocking collectives, per_device(): value_piece_a = lax.all_gather(value_a, 'sp', axis=0, tiled=True)  31.5 us
    all_gather x1, blocking collectives, per_device(): value_piece_b = lax.all_gather(value_b, 'sp', axis=0, tiled=True)  31.4 us
    dot_general x2, matrix products, swiglu_rows(): return jnp.dot(hidden, w_down, preferred_element_type=jnp.float32)  13.8 us
    dot_general x4, matrix products, online_update(): jnp.einsum('qhd,khd->hqk', query_map, key_map, preferred_element_type=jnp...  8.17 us
  transfers between devices with their start and end apart: 4, of which 3 were waited for; matrix products, arithmetic and copies ran while one was open for 3% of the time, Pallas kernels for 0%

commit v1 on v0

v1 whole, which is shorter than its diff:
```python
import jax
import jax.numpy as jnp
from jax import lax
from jax.experimental import pallas as pl
from jax.experimental.pallas import tpu as pltpu
from jax.sharding import PartitionSpec as P

NEG_FILL = -1e30
EPSILON = 1e-05
HEAD_SCALE = 0.8
MAPS = 4


def attend_kernel(
    factor_ref, query_ref, key_ref, value_ref, out_ref, *, chunk, rows, block, tok_dev, part
):
    split = factor_ref[0, 0].astype(jnp.int32)
    scaling = factor_ref[0, 1]
    factor = factor_ref[0, 2]
    total = query_ref.shape[0]
    for begin in range(0, total, chunk):
        sources = chunk // rows
        first = begin // rows
        span = (first + sources) * block
        query = query_ref[begin : begin + chunk, :]
        scores = (
            lax.dot_general(
                query,
                key_ref[:span, :],
                (((1,), (1,)), ((), ())),
                preferred_element_type=jnp.float32,
            )
            * scaling
        )
        row = lax.broadcasted_iota(jnp.int32, (chunk, 1), 0)
        inner = row % rows
        pos = (first + row // rows) * block + (inner // part) * tok_dev + split * part + inner % part
        key_pos = lax.broadcasted_iota(jnp.int32, (chunk, span), 1)
        causal = key_pos <= pos
        scores = jnp.where(causal, scores, NEG_FILL)
        top = jnp.max(scores, axis=1, keepdims=True)
        exponent = jnp.exp(scores - top)
        denom = jnp.sum(exponent, axis=1, keepdims=True)
        numer = jnp.dot(
            exponent.astype(jnp.bfloat16), value_ref[:span, :], preferred_element_type=jnp.float32
        )
        out_ref[begin : begin + chunk, :] = (numer * (factor / denom)).astype(jnp.bfloat16)


def swiglu_rows(row_set, w_gate, w_up, w_down):
    gate_val = jnp.dot(row_set, w_gate, preferred_element_type=jnp.float32)
    up_val = jnp.dot(row_set, w_up, preferred_element_type=jnp.float32)
    hidden = (jax.nn.silu(gate_val) * up_val).astype(jnp.bfloat16)
    return jnp.dot(hidden, w_down, preferred_element_type=jnp.float32)


def widen(array, width):
    return jnp.pad(array, ((0, 0), (0, width - array.shape[1])))


def attention(
    query_a, key_a, value_a, query_b, key_b, value_b, lambda_a, lambda_b, head_gain, tok_dev
):
    sp_count = lax.axis_size("sp")
    tp_count = lax.axis_size("tp")
    splits = sp_count // MAPS
    block = query_a.shape[0]
    width_a, width_b = query_a.shape[2] // 2, query_b.shape[2] // 2
    width = max(width_a, width_b)
    value_width = value_a.shape[2]
    part = tok_dev // splits
    rows = block // splits

    def by_map(array_a, array_b):
        array_a, array_b = array_a[:, 0], array_b[:, 0]
        return [
            widen(array_a[:, :width_a], width),
            widen(array_a[:, width_a:], width),
            array_b[:, :width_b],
            array_b[:, width_b:],
        ]

    keys = by_map(key_a, key_b)
    queries = by_map(query_a, query_b)
    values = [value_a[:, 0]] * 2 + [value_b[:, 0]] * 2
    pieces = []
    for unit in range(MAPS):
        shares = queries[unit].reshape(tp_count, splits, part, width)
        for split in range(splits):
            pieces.append(
                jnp.concatenate(
                    [keys[unit], values[unit], shares[:, split].reshape(rows, width)], axis=0
                )
            )
    packed = jnp.stack(pieces)
    got = lax.all_to_all(packed, "sp", split_axis=0, concat_axis=0, tiled=True)
    key_all = got[:, :block].reshape(-1, width)
    value_all = got[:, block : 2 * block].reshape(-1, value_width)
    query_all = got[:, 2 * block :].reshape(-1, width)
    place = lax.axis_index("sp")
    unit, split = place // splits, place % splits
    in_a = unit < 2
    scaling = jnp.where(in_a, width_a ** (-0.5), width_b ** (-0.5))
    lam = jnp.where(in_a, lambda_a[0], lambda_b[0])
    factor = jnp.where(unit % 2 == 1, lam, 1.0)
    scalars = jnp.stack([split.astype(jnp.float32), scaling, factor])[None]
    total = query_all.shape[0]
    chunk = rows * max(1, min(sp_count, 256 // rows))
    outs = pl.pallas_call(
        lambda *refs: attend_kernel(
            *refs, chunk=chunk, rows=rows, block=block, tok_dev=tok_dev, part=part
        ),
        out_shape=jax.ShapeDtypeStruct((total, value_width), jnp.bfloat16),
        in_specs=[pl.BlockSpec(memory_space=pltpu.SMEM)]
        + [pl.BlockSpec(memory_space=pltpu.VMEM)] * 3,
        out_specs=pl.BlockSpec(memory_space=pltpu.VMEM),
        name="attend",
    )(scalars, query_all, key_all, value_all)
    back = lax.all_to_all(
        outs.reshape(sp_count * tp_count, part, value_width),
        ("sp", "tp"),
        split_axis=0,
        concat_axis=0,
        tiled=True,
    )
    back = back.reshape(2, 2, splits, tp_count, part, value_width).astype(jnp.float32)
    differ = back[:, 0] - back[:, 1]
    scale_rms = lax.rsqrt(jnp.mean(differ * differ, axis=-1, keepdims=True) + EPSILON)
    heads = (differ * scale_rms * head_gain * HEAD_SCALE).astype(jnp.bfloat16)
    return jnp.transpose(heads, (1, 3, 0, 2, 4)).reshape(tok_dev, -1)


def per_device(
    resid,
    query_a,
    key_a,
    value_a,
    query_b,
    key_b,
    value_b,
    lambda_a,
    lambda_b,
    head_gain,
    out_weight,
    norm_gain,
    expert_ids,
    expert_mix,
    gate_experts,
    up_experts,
    down_experts,
    shared_gate,
    shared_up,
    shared_down,
):
    tok_dev = resid.shape[0]
    joined = attention(
        query_a, key_a, value_a, query_b, key_b, value_b, lambda_a, lambda_b, head_gain, tok_dev
    )
    project = jnp.dot(joined, out_weight, preferred_element_type=jnp.float32)
    middle = (resid.astype(jnp.float32) + project).astype(jnp.bfloat16)
    middle_f = middle.astype(jnp.float32)
    normed = (
        middle_f
        * lax.rsqrt(jnp.mean(middle_f * middle_f, axis=1, keepdims=True) + EPSILON)
        * norm_gain[None, :]
    ).astype(jnp.bfloat16)
    shared = swiglu_rows(normed, shared_gate, shared_up, shared_down)
    top_count = expert_ids.shape[1]
    model_width = normed.shape[1]
    sp_count = lax.axis_size("sp")
    tp_count = lax.axis_size("tp")
    expert_total = sp_count * tp_count
    pair_count = tok_dev * top_count
    capacity = max(2, 2 * pair_count // expert_total)
    hits = expert_ids[:, :, None] == jnp.arange(expert_total, dtype=jnp.int32)
    named = jnp.any(hits, axis=1).astype(jnp.float32)
    mixes = jnp.sum(jnp.where(hits, expert_mix[:, :, None], 0.0), axis=1)
    earlier = jnp.tril(jnp.ones((tok_dev, tok_dev), jnp.float32), -1)
    rank = jnp.dot(earlier, named)
    slots = jnp.arange(capacity, dtype=jnp.float32)
    picks = (rank.T[:, None, :] == slots[None, :, None]) & (named.T[:, None, :] > 0)
    pick_rows = picks.astype(jnp.bfloat16).reshape(expert_total * capacity, tok_dev)
    send_rows = (
        jnp.dot(pick_rows, normed, preferred_element_type=jnp.float32)
        .astype(jnp.bfloat16)
        .reshape(expert_total, capacity, model_width)
    )
    arrived = lax.all_to_all(send_rows, ("sp", "tp"), split_axis=0, concat_axis=0, tiled=True)
    arrived_shape = arrived.shape
    flat_rows = arrived.reshape(-1, arrived_shape[-1])
    result = swiglu_rows(flat_rows, gate_experts[0], up_experts[0], down_experts[0]).astype(
        jnp.bfloat16
    )
    finished = result.reshape(arrived_shape)
    returned = lax.all_to_all(finished, ("sp", "tp"), split_axis=0, concat_axis=0, tiled=True)
    mix_picks = jnp.where(
        (rank[:, :, None] == slots) & (named[:, :, None] > 0), mixes[:, :, None], 0.0
    ).reshape(tok_dev, -1)
    mix_high = mix_picks.astype(jnp.bfloat16)
    mix_low = (mix_picks - mix_high.astype(jnp.float32)).astype(jnp.bfloat16)
    both = jnp.dot(
        jnp.concatenate([mix_high, mix_low], axis=0),
        returned.reshape(-1, model_width),
        preferred_element_type=jnp.float32,
    )
    routed = both[:tok_dev] + both[tok_dev:]
    return (middle_f + shared + routed).astype(jnp.bfloat16)


def solution(mesh):
    in_specs = (
        P(("sp", "tp"), None),
        P("sp", "tp", None),
        P("sp", "tp", None),
        P("sp", "tp", None),
        P("sp", "tp", None),
        P("sp", "tp", None),
        P("sp", "tp", None),
        P("tp"),
        P("tp"),
        P(),
        P(),
        P(),
        P(("sp", "tp"), None),
        P(("sp", "tp"), None),
        P(("sp", "tp"), None, None),
        P(("sp", "tp"), None, None),
        P(("sp", "tp"), None, None),
        P(),
        P(),
        P(),
    )
    out_specs = P(("sp", "tp"), None)
    return jax.shard_map(
        per_device, mesh=mesh, in_specs=in_specs, out_specs=out_specs, check_vma=False
    )
```

time: 336 us -> 202 us (0.60)
  blocking collectives: 150 us -> 50.9 us
  local copies, waits for them, and re-layouts: 63.9 us -> 7.04 us
  waiting for transfers between devices: 53.1 us -> 85.8 us
  between operations: 15.1 us -> 1.55 us
  matrix products: 33.6 us -> 27.1 us
  Pallas kernels: 0 us -> 4.7 us
  starting transfers between devices: 10.4 us -> 14.8 us
    all_gather x3 -> x0, blocking collectives: 96.5 us -> none  [the longest x1 33.6 us: per_device(): key_piece_a = lax.all_gather(key_a, 'sp', axis=0, tiled=True)]
    scatter x1 -> x0, local copies, waits for them, and re-layouts: 46.3 us -> none  [per_device(): send_rows = jnp.zeros((expert_total, capacity, model_width), jnp.bfloat16...]
    all_to_all x2, waiting for transfers between devices: 6.5 us -> 39.6 us  [the longest x1 29.4 us: attention(): got = lax.all_to_all(packed, 'sp', split_axis=0, concat_axis=0, tiled=True)]
    gather x2 -> x0, local copies, waits for them, and re-layouts: 7.49 us -> none  [the longest x1 5.15 us: per_device(): returned[flat_ids, pair_rank].reshape(tok_dev, top_count, model_width)]
    dot_general x8 -> x3, matrix products: 10.9 us -> 4.07 us  [the longest x1 3.12 us: per_device(): jnp.dot(jnp.concatenate([mix_high, mix_low], axis=0), returned.reshape(-1...]
    unnamed x0 -> x7, other arithmetic: none -> 5.55 us
    slice x0 -> x10, local copies, waits for them, and re-layouts: none -> 5.42 us  [the longest x2 1.85 us: by_map(): array_a[:, width_a:]]
    reduce_sum x3 -> x2, other arithmetic: 5.36 us -> 0.17 us  [the longest x1 0.15 us: attention(): jnp.mean(differ * differ, axis=-1, keepdims=True) + EPSILON]
  transfers between devices with their start and end apart: 4 -> 3, of which waited for: 3 -> 3; matrix products, arithmetic and copies ran while one was open for 3% -> 2% of each run, Pallas kernels for 0% -> 0%
where the time goes in v1:
time: 202 us; the launch traced here: 201 us
  waiting for transfers between devices  85.8 us (42%)
  blocking collectives  50.9 us (25%)
  matrix products  27.1 us (13%)
  starting transfers between devices  14.8 us (7%)
  other arithmetic  9.52 us (5%)
  local copies, waits for them, and re-layouts  7.04 us (3%)
  Pallas kernels  4.7 us (2%)
    all_to_all x1, blocking collectives, per_device(): lax.all_to_all(send_rows, ('sp', 'tp'), split_axis=0, concat_axis=0, tile...  50.9 us
    all_to_all x1, waiting for transfers between devices, per_device(): lax.all_to_all(finished, ('sp', 'tp'), split_axis=0, concat_axis=0, tiled...  46.3 us
    all_to_all x1, waiting for transfers between devices, attention(): got = lax.all_to_all(packed, 'sp', split_axis=0, concat_axis=0, tiled=True)  29.4 us
    dot_general x2, matrix products, swiglu_rows(): return jnp.dot(hidden, w_down, preferred_element_type=jnp.float32)  14.1 us
    all_to_all x1, waiting for transfers between devices, attention(): lax.all_to_all(outs.reshape(sp_count * tp_count, part, value_width), ('sp...  10.2 us
    all_to_all x1, starting transfers between devices, attention(): got = lax.all_to_all(packed, 'sp', split_axis=0, concat_axis=0, tiled=True)  7.32 us
    dot_general x2, matrix products, swiglu_rows(): gate_val = jnp.dot(row_set, w_gate, preferred_element_type=jnp.float32)  5.77 us
    unnamed x7, other arithmetic  5.55 us
  transfers between devices with their start and end apart: 3, of which 3 were waited for; matrix products, arithmetic and copies ran while one was open for 2% of the time, Pallas kernels for 0%

profile of v1, /device:TPU:0, one launch (start us, length us, event | category | flops | bytes accessed | tf_op | source)
XLA Modules:
  0.0 201.3 jit_solution(14223692041554588687)
XLA Ops:
  0.0 1.0 copy_select_fusion
  1.0 0.9 broadcast_select_fusion
  1.9 0.9 slice.91
  2.9 0.9 slice.90
  3.8 0.9 fusion.59
  4.7 0.9 fusion.58
  5.6 1.5 fusion.25
  7.1 0.7 fusion.26
  7.8 0.7 fusion.27
  8.5 0.7 fusion.28
  9.1 0.7 fusion.29
  9.8 0.7 fusion.30
  10.5 0.7 fusion.31
  11.2 0.7 fusion.32
  11.9 7.3 %all-to-all-start = ((bf16[8,640,128]{2,1,0:T(8,128)(2,1)}), bf16[8,640,128]{2,1,0:T(8,128)(2,1)S(1)}, u32[]{:S(2)}, u32[]{:S(2)}) async-start(bf16[8,640,128]{2,1,0:T(8,128)(2,1)} %fusion.32), calls=%async_computation | async-start | bytes 2621440 | tf_op jit(solution)/shard_map/all_to_all | solution.py:96
  21.2 29.4 %all-to-all-done = bf16[8,640,128]{2,1,0:T(8,128)(2,1)S(1)} async-done(((bf16[8,640,128]{2,1,0:T(8,128)(2,1)}), bf16[8,640,128]{2,1,0:T(8,128)(2,1)S(1)}, u32[]{:S(2)}, u32[]{:S(2)}) %all-to-all-start) | async-done | bytes 1310752 | tf_op jit(solution)/shard_map/all_to_all | solution.py:96
  50.6 0.7 slice.102
  51.3 1.0 fusion.57
  52.3 4.7 %attend.1 = bf16[1024,128]{1,0:T(8,128)(2,1)} custom-call(f32[1,3]{1,0:T(1,128)} %maximum_bitcast_fusion.8.refs_0_, bf16[1024,128]{1,0:T(8,128)(2,1)} %bitcast.168, bf16[2048,128]{1,0:T(8,128)(2,1)} %bitcast.158, bf16[2048,128]{1,0:T(8,128)(2,1)} %bitcast.157), custom_call_target="tpu_custom_call" | custom-call | tf_op jit(solution)/shard_map/attend/pallas_call | solution.py:109
  57.0 3.6 %all-to-all-start.1 = ((bf16[32,32,128]{2,1,0:T(8,128)(2,1)}), bf16[32,32,128]{2,1,0:T(8,128)(2,1)S(1)}, u32[]{:S(2)}, u32[]{:S(2)}) async-start(bf16[32,32,128]{2,1,0:T(8,128)(2,1)} %bitcast.167), calls=%async_computation.1 | async-start | bytes 524288 | tf_op jit(solution)/shard_map/all_to_all | solution.py:119
  61.1 10.2 %all-to-all-done.1 = bf16[32,32,128]{2,1,0:T(8,128)(2,1)S(1)} async-done(((bf16[32,32,128]{2,1,0:T(8,128)(2,1)}), bf16[32,32,128]{2,1,0:T(8,128)(2,1)S(1)}, u32[]{:S(2)}, u32[]{:S(2)}) %all-to-all-start.1) | async-done | bytes 262176 | tf_op jit(solution)/shard_map/all_to_all | solution.py:119
  71.8 3.2 %multiply_reduce_fusion = (f32[64]{0:T(128)S(1)}, f32[64,2048]{1,0:T(8,128)S(1)}) fusion(bf16[64,1024]{1,0:T(8,128)(2,1)S(1)} %reshape.92, bf16[1024,2048]{1,0:T(8,128)(2,1)} %param.30, bf16[64,2048]{1,0:T(8,128)(2,1)S(1)} %copy-done.4), kind=kOutput, calls=%fused_computation.19 | convolution fusion | flops 269221824 | bytes 5112064 | tf_op jit(solution)/shard_map/dot_general | solution.py:159
  75.0 0.8 convolution_convert_fusion
  75.8 50.9 %all_to_all.20 = bf16[32,16,2048]{2,1,0:T(8,128)(2,1)S(1)} all-to-all(bf16[32,16,2048]{2,1,0:T(8,128)(2,1)S(1)} %bitcast.153), channel_id=1, replica_groups=mesh['sp'=8,'tp'=4] {'sp','tp'}, dimensions={0} | all-to-all | bytes 4194304 | tf_op jit(solution)/shard_map/all_to_all | solution.py:188
  126.7 1.3 copy-done.1
  128.0 3.7 %fusion.4 = f32[512,1024]{1,0:T(8,128)} fusion(bf16[512,2048]{1,0:T(8,128)(2,1)S(1)} %bitcast.155, bf16[1,2048,1024]{2,1,0:T(8,128)(2,1)S(1)} %copy-done.9), kind=kOutput, calls=%fused_computation.4 | convolution fusion | flops 2147483648 | bytes 8388608 | tf_op jit(solution)/shard_map/dot_general | solution.py:51
  131.6 10.6 %fusion.6 = bf16[512,2048]{1,0:T(8,128)(2,1)} fusion(bf16[1,1024,2048]{2,1,0:T(8,128)(2,1)} %param.36, f32[512,1024]{1,0:T(8,128)} %fusion.4, bf16[512,2048]{1,0:T(8,128)(2,1)} %bitcast.156, bf16[1,2048,1024]{2,1,0:T(8,128)(2,1)} %param.35), kind=kOutput, calls=%fused_computation.6 | convolution fusion | flops 4299161600 | bytes 14680064 | tf_op jit(solution)/shard_map/dot_general | solution.py:54
  142.2 3.8 %all-to-all-start.3 = ((bf16[32,16,2048]{2,1,0:T(8,128)(2,1)}), bf16[32,16,2048]{2,1,0:T(8,128)(2,1)}, u32[]{:S(2)}, u32[]{:S(2)}) async-start(bf16[32,16,2048]{2,1,0:T(8,128)(2,1)} %bitcast.154), calls=%async_computation.3 | async-start | bytes 4194304 | tf_op jit(solution)/shard_map/all_to_all | solution.py:195
  146.3 2.1 %fusion.56 = f32[64,512]{1,0:T(8,128)S(1)} fusion(bf16[2048,512]{1,0:T(8,128)(2,1)} %param.37, f32[64,2048]{1,0:T(8,128)S(1)} %get-tuple-element.22, f32[2048]{0:T(1024)S(1)} %copy-done.5, f32[64]{0:T(128)S(1)} %add_rsqrt_fusion.1), kind=kOutput, calls=%fused_computation.88 | convolution fusion | flops 134610944 | bytes 2760960 | tf_op jit(solution)/shard_map/dot_general | solution.py:51
  148.4 46.3 %all-to-all-done.3 = bf16[32,16,2048]{2,1,0:T(8,128)(2,1)} async-done(((bf16[32,16,2048]{2,1,0:T(8,128)(2,1)}), bf16[32,16,2048]{2,1,0:T(8,128)(2,1)}, u32[]{:S(2)}, u32[]{:S(2)}) %all-to-all-start.3) | async-done | bytes 2097184 | tf_op jit(solution)/shard_map/all_to_all | solution.py:195
  194.7 3.1 %fusion.34 = f32[128,2048]{1,0:T(8,128)} fusion(bf16[512,2048]{1,0:T(8,128)(2,1)} %bitcast.53, bf16[64,512]{0,1:T(8,128)(2,1)S(1)} %fusion.22, bf16[64,512]{0,1:T(8,128)(2,1)S(1)} %fusion.21), kind=kOutput, calls=%fused_computation.55 | convolution fusion | flops 268697600 | bytes 3276800 | tf_op jit(solution)/shard_map/dot_general | solution.py:201
  197.8 3.5 %fusion.10 = bf16[64,2048]{1,0:T(8,128)(2,1)} fusion(f32[64,2048]{1,0:T(8,128)S(1)} %get-tuple-element.22, bf16[512,2048]{1,0:T(8,128)(2,1)S(1)} %copy-done, bf16[2048,512]{1,0:T(8,128)(2,1)} %param.38, f32[128,2048]{1,0:T(8,128)} %fusion.34, f32[64,512]{1,0:T(8,128)S(1)} %fusion.56, f32[2048]{0:T(1024)S(1)} %copy-done.5, f32[64]{0:T(128)S(1)} %add_rsqrt_fusion.1), kind=kOutput, calls=%fused_computation.11 | convolution fusion | flops 269549568 | bytes 6693376 | tf_op jit(solution)/shard_map/dot_general | solution.py:54
  (42 shorter events, 1.9 us)
Async XLA Ops:
  0.0 197.8 %copy-start = (bf16[512,2048]{1,0:T(8,128)(2,1)S(1)}, bf16[512,2048]{1,0:T(8,128)(2,1)}, u32[]{:S(2)}) copy-start(bf16[512,2048]{1,0:T(8,128)(2,1)} %param.39) | copy-start | bytes 6291460
  0.0 7.1 %copy-start.2 = (bf16[256,1,128]{2,0,1:T(8,128)(2,1)S(1)}, bf16[256,1,128]{2,0,1:T(8,128)(2,1)}, u32[]{:S(2)}) copy-start(bf16[256,1,128]{2,0,1:T(8,128)(2,1)} %param.23) | copy-start | bytes 196612
  0.0 9.1 %copy-start.3 = (bf16[256,1,128]{2,0,1:T(8,128)(2,1)S(1)}, bf16[256,1,128]{2,0,1:T(8,128)(2,1)}, u32[]{:S(2)}) copy-start(bf16[256,1,128]{2,0,1:T(8,128)(2,1)} %param.26) | copy-start | bytes 196612
  9.1 12.0 %copy-start.6 = (s32[64,4]{0,1:T(4,128)S(1)}, s32[64,4]{0,1:T(4,128)}, u32[]{:S(2)}) copy-start(s32[64,4]{0,1:T(4,128)} %param.32) | copy-start | bytes 3076
  11.9 38.7 %all-to-all-start = ((bf16[8,640,128]{2,1,0:T(8,128)(2,1)}), bf16[8,640,128]{2,1,0:T(8,128)(2,1)S(1)}, u32[]{:S(2)}, u32[]{:S(2)}) async-start(bf16[8,640,128]{2,1,0:T(8,128)(2,1)} %fusion.32), calls=%async_computation | async-start | bytes 2621440 | tf_op jit(solution)/shard_map/all_to_all | solution.py:96
  52.3 19.2 %copy-start.8 = (f32[128]{0:T(128)S(1)}, f32[128]{0:T(128)}, u32[]{:S(2)}) copy-start(f32[128]{0:T(128)} %param.29) | copy-start | bytes 1540
  52.3 19.5 %copy-start.4 = (bf16[64,2048]{1,0:T(8,128)(2,1)S(1)}, bf16[64,2048]{1,0:T(8,128)(2,1)}, u32[]{:S(2)}) copy-start(bf16[64,2048]{1,0:T(8,128)(2,1)} %param.20) | copy-start | bytes 786436
  57.0 14.2 %all-to-all-start.1 = ((bf16[32,32,128]{2,1,0:T(8,128)(2,1)}), bf16[32,32,128]{2,1,0:T(8,128)(2,1)S(1)}, u32[]{:S(2)}, u32[]{:S(2)}) async-start(bf16[32,32,128]{2,1,0:T(8,128)(2,1)} %bitcast.167), calls=%async_computation.1 | async-start | bytes 524288 | tf_op jit(solution)/shard_map/all_to_all | solution.py:119
  71.8 3.2 %copy-start.5 = (f32[2048]{0:T(1024)S(1)}, f32[2048]{0:T(1024)}, u32[]{:S(2)}) copy-start(f32[2048]{0:T(1024)} %param.31) | copy-start | bytes 24580
  75.8 52.2 %copy-start.9 = (bf16[1,2048,1024]{2,1,0:T(8,128)(2,1)S(1)}, bf16[1,2048,1024]{2,1,0:T(8,128)(2,1)}, u32[]{:S(2)}) copy-start(bf16[1,2048,1024]{2,1,0:T(8,128)(2,1)} %param.34) | copy-start | bytes 12582916
  126.7 1.3 copy-start.1
  142.2 3.8 %copy-start.7 = (f32[64,4]{0,1:T(4,128)S(1)}, f32[64,4]{0,1:T(4,128)}, u32[]{:S(2)}) copy-start(f32[64,4]{0,1:T(4,128)} %param.33) | copy-start | bytes 3076
  142.2 52.5 %all-to-all-start.3 = ((bf16[32,16,2048]{2,1,0:T(8,128)(2,1)}), bf16[32,16,2048]{2,1,0:T(8,128)(2,1)}, u32[]{:S(2)}, u32[]{:S(2)}) async-start(bf16[32,16,2048]{2,1,0:T(8,128)(2,1)} %bitcast.154), calls=%async_computation.3 | async-start | bytes 4194304 | tf_op jit(solution)/shard_map/all_to_all | solution.py:195

commit v2 on v1

--- a/solution.py
+++ b/solution.py
@@ -12,21 +12,22 @@
 
 
 def attend_kernel(
-    factor_ref, query_ref, key_ref, value_ref, out_ref, *, chunk, rows, block, tok_dev, part
+    factor_ref, got_ref, out_ref, *, chunk, rows, block, tok_dev, part
 ):
     split = factor_ref[0, 0].astype(jnp.int32)
     scaling = factor_ref[0, 1]
     factor = factor_ref[0, 2]
-    total = query_ref.shape[0]
-    for begin in range(0, total, chunk):
-        sources = chunk // rows
-        first = begin // rows
-        span = (first + sources) * block
-        query = query_ref[begin : begin + chunk, :]
+    width = got_ref.shape[2]
+    sources = chunk // rows
+    for first in range(0, got_ref.shape[0], sources):
+        begin = first * rows
+        last = first + sources
+        span = last * block
+        query = got_ref[first:last, 2 * block :, :].reshape(chunk, width)
         scores = (
             lax.dot_general(
                 query,
-                key_ref[:span, :],
+                got_ref[:last, :block, :].reshape(span, width),
                 (((1,), (1,)), ((), ())),
                 preferred_element_type=jnp.float32,
             )
@@ -42,7 +43,9 @@
         exponent = jnp.exp(scores - top)
         denom = jnp.sum(exponent, axis=1, keepdims=True)
         numer = jnp.dot(
-            exponent.astype(jnp.bfloat16), value_ref[:span, :], preferred_element_type=jnp.float32
+            exponent.astype(jnp.bfloat16),
+            got_ref[:last, block : 2 * block, :].reshape(span, width),
+            preferred_element_type=jnp.float32,
         )
         out_ref[begin : begin + chunk, :] = (numer * (factor / denom)).astype(jnp.bfloat16)
 
@@ -54,8 +57,88 @@
     return jnp.dot(hidden, w_down, preferred_element_type=jnp.float32)
 
 
-def widen(array, width):
-    return jnp.pad(array, ((0, 0), (0, width - array.shape[1])))
+def pack_kernel(qa_ref, ka_ref, va_ref, qb_ref, kb_ref, vb_ref, out_ref, *, splits, tok_dev):
+    block = ka_ref.shape[0]
+    width = out_ref.shape[2]
+    part = tok_dev // splits
+    half = width // 2
+    lane = lax.broadcasted_iota(jnp.int32, (block, width), 1)
+    query_a = qa_ref[...]
+    zero = jnp.zeros_like(query_a)
+    queries = [
+        jnp.where(lane < half, query_a, zero),
+        jnp.where(lane >= half, query_a, zero),
+        qb_ref[:, :width],
+        qb_ref[:, width:],
+    ]
+    keys = [ka_ref[...], ka_ref[...], kb_ref[:, :width], kb_ref[:, width:]]
+    values = [va_ref[...], va_ref[...], vb_ref[...], vb_ref[...]]
+    for unit in range(MAPS):
+        for split in range(splits):
+            piece = unit * splits + split
+            out_ref[piece, :block, :] = keys[unit]
+            out_ref[piece, block : 2 * block, :] = values[unit]
+            shares = queries[unit].reshape(block // tok_dev, splits, part, width)[:, split]
+            out_ref[piece, 2 * block :, :] = shares.reshape(block // splits, width)
+
+
+def expert_kernel(row_ref, gate_ref, up_ref, down_ref, out_ref, sum_ref):
+    rows = row_ref[...]
+    gate_val = jnp.dot(rows, gate_ref[...], preferred_element_type=jnp.float32)
+    up_val = jnp.dot(rows, up_ref[...], preferred_element_type=jnp.float32)
+    hidden = (gate_val * jax.nn.sigmoid(gate_val) * up_val).astype(jnp.bfloat16)
+    result = jnp.dot(hidden, down_ref[...], preferred_element_type=jnp.float32)
+    last = pl.num_programs(0) - 1
+
+    @pl.when(pl.program_id(0) == 0)
+    def _():
+        sum_ref[...] = result
+
+    @pl.when((pl.program_id(0) > 0) & (pl.program_id(0) < last))
+    def _():
+        sum_ref[...] += result
+
+    @pl.when(pl.program_id(0) == last)
+    def _():
+        out_ref[...] = (sum_ref[...] + result).astype(jnp.bfloat16)
+
+
+def expert_call(rows, w_gate, w_up, w_down):
+    count, model_width = rows.shape
+    hidden_width = w_gate.shape[1]
+    step = hidden_width // 4
+    return pl.pallas_call(
+        expert_kernel,
+        grid=(4,),
+        out_shape=jax.ShapeDtypeStruct(rows.shape, jnp.bfloat16),
+        in_specs=[
+            pl.BlockSpec((count, model_width), lambda i: (0, 0)),
+            pl.BlockSpec((model_width, step), lambda i: (0, i)),
+            pl.BlockSpec((model_width, step), lambda i: (0, i)),
+            pl.BlockSpec((step, model_width), lambda i: (i, 0)),
+        ],
+        out_specs=pl.BlockSpec((count, model_width), lambda i: (0, 0)),
+        scratch_shapes=[pltpu.VMEM((count, model_width), jnp.float32)],
+        name="expert",
+    )(rows, w_gate, w_up, w_down)
+
+
+def combine_kernel(mix_ref, row_ref, base_ref, out_ref):
+    tokens = base_ref.shape[0]
+    both = jnp.dot(mix_ref[...], row_ref[...], preferred_element_type=jnp.float32)
+    out_ref[...] = (base_ref[...] + (both[:tokens] + both[tokens:])).astype(jnp.bfloat16)
+
+
+def local_call(kernel, shape, name, operands, scalars=0):
+    specs = [pl.BlockSpec(memory_space=pltpu.SMEM)] * scalars
+    specs += [pl.BlockSpec(memory_space=pltpu.VMEM)] * (len(operands) - scalars)
+    return pl.pallas_call(
+        kernel,
+        out_shape=jax.ShapeDtypeStruct(shape, jnp.bfloat16),
+        in_specs=specs,
+        out_specs=pl.BlockSpec(memory_space=pltpu.VMEM),
+        name=name,
+    )(*operands)
 
 
 def attention(
@@ -71,32 +154,17 @@
     part = tok_dev // splits
     rows = block // splits
 
-    def by_map(array_a, array_b):
-        array_a, array_b = array_a[:, 0], array_b[:, 0]
-        return [
-            widen(array_a[:, :width_a], width),
-            widen(array_a[:, width_a:], width),
-            array_b[:, :width_b],
-            array_b[:, width_b:],
-        ]
-
-    keys = by_map(key_a, key_b)
-    queries = by_map(query_a, query_b)
-    values = [value_a[:, 0]] * 2 + [value_b[:, 0]] * 2
-    pieces = []
-    for unit in range(MAPS):
-        shares = queries[unit].reshape(tp_count, splits, part, width)
-        for split in range(splits):
-            pieces.append(
-                jnp.concatenate(
-                    [keys[unit], values[unit], shares[:, split].reshape(rows, width)], axis=0
-                )
-            )
-    packed = jnp.stack(pieces)
+    flat = [
+        array.reshape(block, array.shape[2])
+        for array in (query_a, key_a, value_a, query_b, key_b, value_b)
+    ]
+    packed = local_call(
+        lambda *refs: pack_kernel(*refs, splits=splits, tok_dev=tok_dev),
+        (sp_count, 2 * block + rows, width),
+        "pack",
+        flat,
+    )
     got = lax.all_to_all(packed, "sp", split_axis=0, concat_axis=0, tiled=True)
-    key_all = got[:, :block].reshape(-1, width)
-    value_all = got[:, block : 2 * block].reshape(-1, value_width)
-    query_all = got[:, 2 * block :].reshape(-1, width)
     place = lax.axis_index("sp")
     unit, split = place // splits, place % splits
     in_a = unit < 2
@@ -104,18 +172,17 @@
     lam = jnp.where(in_a, lambda_a[0], lambda_b[0])
     factor = jnp.where(unit % 2 == 1, lam, 1.0)
     scalars = jnp.stack([split.astype(jnp.float32), scaling, factor])[None]
-    total = query_all.shape[0]
+    total = sp_count * rows
     chunk = rows * max(1, min(sp_count, 256 // rows))
-    outs = pl.pallas_call(
+    outs = local_call(
         lambda *refs: attend_kernel(
             *refs, chunk=chunk, rows=rows, block=block, tok_dev=tok_dev, part=part
         ),
-        out_shape=jax.ShapeDtypeStruct((total, value_width), jnp.bfloat16),
-        in_specs=[pl.BlockSpec(memory_space=pltpu.SMEM)]
-        + [pl.BlockSpec(memory_space=pltpu.VMEM)] * 3,
-        out_specs=pl.BlockSpec(memory_space=pltpu.VMEM),
-        name="attend",
-    )(scalars, query_all, key_all, value_all)
+        (total, value_width),
+        "attend",
+        [scalars, got],
+        scalars=1,
+    )
     back = lax.all_to_all(
         outs.reshape(sp_count * tp_count, part, value_width),
         ("sp", "tp"),
@@ -188,9 +255,7 @@
     arrived = lax.all_to_all(send_rows, ("sp", "tp"), split_axis=0, concat_axis=0, tiled=True)
     arrived_shape = arrived.shape
     flat_rows = arrived.reshape(-1, arrived_shape[-1])
-    result = swiglu_rows(flat_rows, gate_experts[0], up_experts[0], down_experts[0]).astype(
-        jnp.bfloat16
-    )
+    result = expert_call(flat_rows, gate_experts[0], up_experts[0], down_experts[0])
     finished = result.reshape(arrived_shape)
     returned = lax.all_to_all(finished, ("sp", "tp"), split_axis=0, concat_axis=0, tiled=True)
     mix_picks = jnp.where(
@@ -198,13 +263,13 @@
     ).reshape(tok_dev, -1)
     mix_high = mix_picks.astype(jnp.bfloat16)
     mix_low = (mix_picks - mix_high.astype(jnp.float32)).astype(jnp.bfloat16)
-    both = jnp.dot(
-        jnp.concatenate([mix_high, mix_low], axis=0),
-        returned.reshape(-1, model_width),
-        preferred_element_type=jnp.float32,
-    )
-    routed = both[:tok_dev] + both[tok_dev:]
-    return (middle_f + shared + routed).astype(jnp.bfloat16)
+    mix_rows = jnp.concatenate([mix_high, mix_low], axis=0)
+    return local_call(
+        combine_kernel,
+        (tok_dev, model_width),
+        "combine",
+        [mix_rows, returned.reshape(-1, model_width), middle_f + shared],
+    )
 
 
 def solution(mesh):

time: 202 us -> 185 us (0.916)
  Pallas kernels: 4.7 us -> 23 us
  matrix products: 27.1 us -> 9.57 us
  other arithmetic: 9.52 us -> 1.89 us
  local copies, waits for them, and re-layouts: 7.04 us -> 1.73 us
  waiting for transfers between devices: 85.8 us -> 81.5 us
    pallas_call x1 -> x4, Pallas kernels: 4.7 us -> 23 us  [the longest x1 13 us: expert_call(): pl.pallas_call(expert_kernel, grid=(4,), out_shape=jax.ShapeDtypeStruct(r...]
    dot_general x2 -> x1, matrix products: 14.1 us -> 3.36 us  [swiglu_rows(): return jnp.dot(hidden, w_down, preferred_element_type=jnp.float32)]
    unnamed x7 -> x0, other arithmetic: 5.55 us -> none
    slice x10 -> x0, local copies, waits for them, and re-layouts: 5.42 us -> none  [the longest x2 1.85 us: by_map(): array_a[:, width_a:]]
    all_to_all x1, waiting for transfers between devices: 46.3 us -> 42 us  [per_device(): lax.all_to_all(finished, ('sp', 'tp'), split_axis=0, concat_axis=0, tiled...]
    dot_general x2 -> x1, matrix products: 5.77 us -> 2.11 us  [swiglu_rows(): gate_val = jnp.dot(row_set, w_gate, preferred_element_type=jnp.float32)]
    dot_general x1 -> x0, matrix products: 3.12 us -> none  [per_device(): jnp.dot(jnp.concatenate([mix_high, mix_low], axis=0), returned.reshape(-1...]
  transfers between devices with their start and end apart: 3 -> 3, of which waited for: 3 -> 3; matrix products, arithmetic and copies ran while one was open for 2% -> 4% of each run, Pallas kernels for 0% -> 0%
where the time goes in v2:
time: 185 us
  waiting for transfers between devices  81.5 us (44%)
  blocking collectives  51.1 us (28%)
  Pallas kernels  23 us (12%)
  starting transfers between devices  14.7 us (8%)
  matrix products  9.57 us (5%)
  other arithmetic  1.89 us (1%)
    all_to_all x1, blocking collectives, per_device(): lax.all_to_all(send_rows, ('sp', 'tp'), split_axis=0, concat_axis=0, tile...  51.1 us
    all_to_all x1, waiting for transfers between devices, per_device(): lax.all_to_all(finished, ('sp', 'tp'), split_axis=0, concat_axis=0, tiled...  42 us
    all_to_all x1, waiting for transfers between devices, attention(): got = lax.all_to_all(packed, 'sp', split_axis=0, concat_axis=0, tiled=True)  29.3 us
    pallas_call x1, Pallas kernels, expert_call(): pl.pallas_call(expert_kernel, grid=(4,), out_shape=jax.ShapeDtypeStruct(r...  13 us
    all_to_all x1, waiting for transfers between devices, attention(): lax.all_to_all(outs.reshape(sp_count * tp_count, part, value_width), ('sp...  10.2 us
    pallas_call x3, Pallas kernels, local_call(): pl.pallas_call(kernel, out_shape=jax.ShapeDtypeStruct(shape, jnp.bfloat16...  10 us
    all_to_all x1, starting transfers between devices, attention(): got = lax.all_to_all(packed, 'sp', split_axis=0, concat_axis=0, tiled=True)  7.31 us
    all_to_all x1, starting transfers between devices, per_device(): lax.all_to_all(finished, ('sp', 'tp'), split_axis=0, concat_axis=0, tiled...  3.72 us
  transfers between devices with their start and end apart: 3, of which 3 were waited for; matrix products, arithmetic and copies ran while one was open for 4% of the time, Pallas kernels for 0%

profile of v2, /device:TPU:0, one launch (start us, length us, event | category | flops | bytes accessed | tf_op | source)
XLA Modules:
  0.0 185.0 jit_solution(17266765300642159590)
XLA Ops:
  0.0 0.0 copy-start
  0.0 2.5 %pack.1 = bf16[8,640,128]{2,1,0:T(8,128)(2,1)} custom-call(bf16[256,128]{1,0:T(8,128)(2,1)} %bitcast.65, bf16[256,128]{1,0:T(8,128)(2,1)} %bitcast.66, bf16[256,128]{1,0:T(8,128)(2,1)} %bitcast.67, bf16[256,256]{1,0:T(8,128)(2,1)} %bitcast.63, bf16[256,256]{1,0:T(8,128)(2,1)} %bitcast.64, bf16[256,128]{1,0:T(8,128)(2,1)} %bitcast.68), custom_call_target="tpu_custom_call" | custom-call | tf_op jit(solution)/shard_map/pack/pallas_call | solution.py:135
  2.5 7.3 %all-to-all-start = ((bf16[8,640,128]{2,1,0:T(8,128)(2,1)}), bf16[8,640,128]{2,1,0:T(8,128)(2,1)S(1)}, u32[]{:S(2)}, u32[]{:S(2)}) async-start(bf16[8,640,128]{2,1,0:T(8,128)(2,1)} %pack.1), calls=%async_computation | async-start | bytes 2621440 | tf_op jit(solution)/shard_map/all_to_all | solution.py:167
  11.1 0.1 eq.65
  11.2 0.6 maximum_bitcast_fusion.refs_0_
  11.8 0.0 copy-done.4
  11.8 29.3 %all-to-all-done.refs_1_ = bf16[8,640,128]{2,1,0:T(8,128)(2,1)S(1)} async-done(((bf16[8,640,128]{2,1,0:T(8,128)(2,1)}), bf16[8,640,128]{2,1,0:T(8,128)(2,1)S(1)}, u32[]{:S(2)}, u32[]{:S(2)}) %all-to-all-start) | async-done | bytes 1310752 | tf_op jit(solution)/shard_map/all_to_all | solution.py:167
  41.2 1.1 copy-done.1
  42.2 4.7 %attend.1 = bf16[1024,128]{1,0:T(8,128)(2,1)} custom-call(f32[1,3]{1,0:T(1,128)} %maximum_bitcast_fusion.refs_0_, bf16[8,640,128]{2,1,0:T(8,128)(2,1)} %copy-done.1), custom_call_target="tpu_custom_call" | custom-call | tf_op jit(solution)/shard_map/attend/pallas_call | solution.py:135
  46.9 3.6 %all-to-all-start.1 = ((bf16[32,32,128]{2,1,0:T(8,128)(2,1)}), bf16[32,32,128]{2,1,0:T(8,128)(2,1)S(1)}, u32[]{:S(2)}, u32[]{:S(2)}) async-start(bf16[32,32,128]{2,1,0:T(8,128)(2,1)} %bitcast.61), calls=%async_computation.1 | async-start | bytes 524288 | tf_op jit(solution)/shard_map/all_to_all | solution.py:186
  50.6 0.2 fusion.13
  50.8 0.1 fusion.4
  50.9 10.2 %all-to-all-done.1 = bf16[32,32,128]{2,1,0:T(8,128)(2,1)S(1)} async-done(((bf16[32,32,128]{2,1,0:T(8,128)(2,1)}), bf16[32,32,128]{2,1,0:T(8,128)(2,1)S(1)}, u32[]{:S(2)}, u32[]{:S(2)}) %all-to-all-start.1) | async-done | bytes 262176 | tf_op jit(solution)/shard_map/all_to_all | solution.py:186
  61.2 0.2 multiply_reduce_fusion.1
  61.3 0.0 copy-done.6
  61.4 0.1 fusion.5
  61.5 0.1 copy.39
  61.6 0.1 reshape.86
  61.7 0.0 copy-start.3
  61.7 3.2 %multiply_reduce_fusion = (f32[64]{0:T(128)S(1)}, f32[64,2048]{1,0:T(8,128)S(1)}) fusion(bf16[64,1024]{1,0:T(8,128)(2,1)S(1)} %reshape.86, bf16[1024,2048]{1,0:T(8,128)(2,1)} %param.30, bf16[64,2048]{1,0:T(8,128)(2,1)S(1)} %copy-done.2), kind=kOutput, calls=%fused_computation.8 | convolution fusion | flops 269221824 | bytes 5112064 | tf_op jit(solution)/shard_map/dot_general | solution.py:226
  64.9 0.8 convolution_convert_fusion
  65.6 51.1 %all_to_all.20 = bf16[32,16,2048]{2,1,0:T(8,128)(2,1)} all-to-all(bf16[32,16,2048]{2,1,0:T(8,128)(2,1)S(1)} %bitcast.53), channel_id=1, replica_groups=mesh['sp'=8,'tp'=4] {'sp','tp'}, dimensions={0} | all-to-all | bytes 4194304 | tf_op jit(solution)/shard_map/all_to_all | solution.py:255
  116.7 13.0 %expert.1 = bf16[512,2048]{1,0:T(8,128)(2,1)} custom-call(bf16[512,2048]{1,0:T(8,128)(2,1)} %bitcast.55, bf16[2048,1024]{1,0:T(8,128)(2,1)} %bitcast.56, bf16[2048,1024]{1,0:T(8,128)(2,1)} %bitcast.57, bf16[1024,2048]{1,0:T(8,128)(2,1)} %bitcast.58), custom_call_target="tpu_custom_call" | custom-call | tf_op jit(solution)/shard_map/expert/pallas_call | solution.py:110
  129.7 3.7 %all-to-all-start.3 = ((bf16[32,16,2048]{2,1,0:T(8,128)(2,1)}), bf16[32,16,2048]{2,1,0:T(8,128)(2,1)}, u32[]{:S(2)}, u32[]{:S(2)}) async-start(bf16[32,16,2048]{2,1,0:T(8,128)(2,1)} %bitcast.54), calls=%async_computation.3 | async-start | bytes 4194304 | tf_op jit(solution)/shard_map/all_to_all | solution.py:260
  133.4 0.1 copy.36
  133.6 0.1 copy.37
  133.7 0.1 copy.38
  134.0 0.7 pad_maximum_fusion.mix_ref
  134.6 2.1 %fusion.23 = f32[64,512]{1,0:T(8,128)S(1)} fusion(bf16[2048,512]{1,0:T(8,128)(2,1)} %param.37, f32[64,2048]{1,0:T(8,128)S(1)} %get-tuple-element.8, f32[2048]{0:T(1024)S(1)} %copy-done.3, f32[64]{0:T(128)S(1)} %add_rsqrt_fusion.1), kind=kOutput, calls=%fused_computation.45 | convolution fusion | flops 134610944 | bytes 2760960 | tf_op jit(solution)/shard_map/dot_general | solution.py:54
  136.7 3.4 %convolution_add_fusion.base_ref = f32[64,2048]{1,0:T(8,128)} fusion(f32[64,2048]{1,0:T(8,128)S(1)} %get-tuple-element.8, bf16[512,2048]{1,0:T(8,128)(2,1)S(1)} %copy-done, bf16[2048,512]{1,0:T(8,128)(2,1)} %param.38, f32[64,512]{1,0:T(8,128)S(1)} %fusion.23, f32[2048]{0:T(1024)S(1)} %copy-done.3, f32[64]{0:T(128)S(1)} %add_rsqrt_fusion.1), kind=kOutput, calls=%fused_computation.1 | convolution fusion | flops 269156352 | bytes 5382400 | tf_op jit(solution)/shard_map/dot_general | solution.py:57
  140.1 42.0 %all-to-all-done.3 = bf16[32,16,2048]{2,1,0:T(8,128)(2,1)} async-done(((bf16[32,16,2048]{2,1,0:T(8,128)(2,1)}), bf16[32,16,2048]{2,1,0:T(8,128)(2,1)}, u32[]{:S(2)}, u32[]{:S(2)}) %all-to-all-start.3) | async-done | bytes 2097184 | tf_op jit(solution)/shard_map/all_to_all | solution.py:260
  182.1 2.9 %combine.1 = bf16[64,2048]{1,0:T(8,128)(2,1)} custom-call(bf16[128,512]{1,0:T(8,128)(2,1)} %pad_maximum_fusion.mix_ref, bf16[512,2048]{1,0:T(8,128)(2,1)} %bitcast.30.row_ref, f32[64,2048]{1,0:T(8,128)} %convolution_add_fusion.base_ref), custom_call_target="tpu_custom_call" | custom-call | tf_op jit(solution)/shard_map/combine/pallas_call | solution.py:135
  (22 shorter events, 0.3 us)
Async XLA Ops:
  0.0 136.7 %copy-start = (bf16[512,2048]{1,0:T(8,128)(2,1)S(1)}, bf16[512,2048]{1,0:T(8,128)(2,1)}, u32[]{:S(2)}) copy-start(bf16[512,2048]{1,0:T(8,128)(2,1)} %param.39) | copy-start | bytes 6291460
  0.0 11.8 %copy-start.4 = (s32[64,4]{0,1:T(4,128)S(1)}, s32[64,4]{0,1:T(4,128)}, u32[]{:S(2)}) copy-start(s32[64,4]{0,1:T(4,128)} %param.32) | copy-start | bytes 3076
  2.5 38.7 %all-to-all-start = ((bf16[8,640,128]{2,1,0:T(8,128)(2,1)}), bf16[8,640,128]{2,1,0:T(8,128)(2,1)S(1)}, u32[]{:S(2)}, u32[]{:S(2)}) async-start(bf16[8,640,128]{2,1,0:T(8,128)(2,1)} %pack.1), calls=%async_computation | async-start | bytes 2621440 | tf_op jit(solution)/shard_map/all_to_all | solution.py:167
  9.8 51.6 %copy-start.6 = (f32[128]{0:T(128)S(1)}, f32[128]{0:T(128)}, u32[]{:S(2)}) copy-start(f32[128]{0:T(128)} %param.29) | copy-start | bytes 1540
  41.2 1.1 copy-start.1
  46.9 14.8 %copy-start.2 = (bf16[64,2048]{1,0:T(8,128)(2,1)S(1)}, bf16[64,2048]{1,0:T(8,128)(2,1)}, u32[]{:S(2)}) copy-start(bf16[64,2048]{1,0:T(8,128)(2,1)} %param.20) | copy-start | bytes 786436
  46.9 14.2 %all-to-all-start.1 = ((bf16[32,32,128]{2,1,0:T(8,128)(2,1)}), bf16[32,32,128]{2,1,0:T(8,128)(2,1)S(1)}, u32[]{:S(2)}, u32[]{:S(2)}) async-start(bf16[32,32,128]{2,1,0:T(8,128)(2,1)} %bitcast.61), calls=%async_computation.1 | async-start | bytes 524288 | tf_op jit(solution)/shard_map/all_to_all | solution.py:186
  61.7 3.2 %copy-start.3 = (f32[2048]{0:T(1024)S(1)}, f32[2048]{0:T(1024)}, u32[]{:S(2)}) copy-start(f32[2048]{0:T(1024)} %param.31) | copy-start | bytes 24580
  129.6 4.0 %copy-start.5 = (f32[64,4]{0,1:T(4,128)S(1)}, f32[64,4]{0,1:T(4,128)}, u32[]{:S(2)}) copy-start(f32[64,4]{0,1:T(4,128)} %param.33) | copy-start | bytes 3076
  129.7 52.4 %all-to-all-start.3 = ((bf16[32,16,2048]{2,1,0:T(8,128)(2,1)}), bf16[32,16,2048]{2,1,0:T(8,128)(2,1)}, u32[]{:S(2)}, u32[]{:S(2)}) async-start(bf16[32,16,2048]{2,1,0:T(8,128)(2,1)} %bitcast.54), calls=%async_computation.3 | async-start | bytes 4194304 | tf_op jit(solution)/shard_map/all_to_all | solution.py:260
